TPU v7x, 32 devices: a whole 2x2x4 slice. The times are simulated.
32 devices in a mesh: grp: 2 (over y), sp: 4 (over z), tp: 4 (over x, core).
Axes of the slice: x: 2, y: 2, z: 4, core: 2. Of those that a mesh axis runs over, the one named last changes fastest.
Arguments:
- latent: bfloat16 [4096, 4096], P(('grp', 'sp'), 'tp'), parts along dimension 0, may hold values from -42 to 42
- context: bfloat16 [2048, 4096], P(('grp', 'sp'), 'tp'), parts along dimension 0, may hold values from -42 to 42
- conditions: float32 [4, 4096], P('grp', 'sp'), parts along dimension 0, may hold values from -6 to 6
- mod_weight: bfloat16 [4096, 3, 4096], P('sp', None, 'tp'), may hold values from -0.09375 to 0.09375
- norm_gain: float32 [4096], P('tp'), may hold values from 0.1 to 1.9
- w_query: bfloat16 [4096, 2048], P(None, 'tp'), may hold values from -0.09375 to 0.09375
- w_key: bfloat16 [4096, 2048], P(None, 'tp'), may hold values from -0.09375 to 0.09375
- w_value: bfloat16 [4096, 2048], P(None, 'tp'), may hold values from -0.09375 to 0.09375
- query_gain: float32 [64], replicated, may hold values from 1 to 14
- key_gain: float32 [64], replicated, may hold values from 1 to 14
- lambdas: float32 [16], P('tp'), may hold values from 0.3 to 0.8
- out_gain: float32 [128], replicated, may hold values from 0.1 to 1.9
- w_out: bfloat16 [2048, 4096], P(None, 'tp'), may hold values from -0.125 to 0.125
Outputs:
- updated: bfloat16 [4096, 4096], P(('grp', 'sp'), 'tp'), parts along dimension 0
There are 2 independent parts, one for each index of `grp`. A program takes and returns all parts, laid end to end along the dimension named above; an argument that names none is the same for every part. Nothing has to cross between parts.
All inputs are finite; a program needn't handle non-finite values.
Results may differ from a plain program's by a relative error of at most 0.0076.
Values may be sent and summed in bfloat16 or wider, within the bound.
A program may use at most 128 MiB of HBM per device.

v0:
```python
import math
import jax
import jax.numpy as jnp
from jax import lax
from jax.sharding import PartitionSpec as P

DK = 64
DV = 128
GRID_W = 64
epsilon = 1e-06


def turn_half(halves, angles):
    quarter = halves.shape[-1] // 2
    cosine = jnp.cos(angles)[:, None, None, :]
    sine_part = jnp.sin(angles)[:, None, None, :]
    first_part = halves[..., :quarter]
    second = halves[..., quarter:]
    return jnp.concatenate(
        [first_part * cosine - second * sine_part, first_part * sine_part + second * cosine],
        axis=-1,
    )


def rotate(features, positions):
    half_width = features.shape[-1] // 2
    quarter = half_width // 2
    inverse = 10000.0 ** (-2.0 * jnp.arange(quarter, dtype=jnp.float32) / half_width)
    grid_row = (positions // GRID_W).astype(jnp.float32)
    grid_column = (positions % GRID_W).astype(jnp.float32)
    return jnp.concatenate(
        [
            turn_half(features[..., :half_width], grid_row[:, None] * inverse),
            turn_half(features[..., half_width:], grid_column[:, None] * inverse),
        ],
        axis=-1,
    )


def head_norm(features, gain_row):
    return (
        features
        * lax.rsqrt(jnp.mean(features * features, axis=-1, keepdims=True) + epsilon)
        * gain_row
    )


def modulate(rows_in, gain_row, shift_row, scale_row):
    floats = rows_in.astype(jnp.float32)
    factor = lax.rsqrt(jnp.mean(floats * floats, axis=1, keepdims=True) + epsilon)
    return (floats * factor * gain_row * (1.0 + scale_row) + shift_row).astype(jnp.bfloat16)


def local(
    latent,
    context,
    conditions,
    mod_weight,
    norm_gain,
    w_query,
    w_key,
    w_value,
    query_gain,
    key_gain,
    lambdas,
    out_gain,
    w_out,
):
    tok_rows = latent.shape[0]
    ctx_rows = context.shape[0]
    columns = latent.shape[1]
    heads_here = lambdas.shape[0]
    in_rows = mod_weight.shape[0]
    activated = jax.nn.silu(conditions).astype(jnp.bfloat16)
    partial_mod = jnp.dot(
        activated, mod_weight.reshape(in_rows, 3 * columns), preferred_element_type=jnp.float32
    ).reshape(2, 3, columns)
    modulation = lax.psum(partial_mod, "sp")
    lat_floats = latent.astype(jnp.float32)
    full_gain, full_pairs = (
        lax.all_gather(norm_gain, "tp", axis=0, tiled=True),
        lax.all_gather(modulation[:, :2], "tp", axis=2, tiled=True),
    )
    whole_lat, whole_ctx = (
        lax.all_gather(latent, "tp", axis=1, tiled=True),
        lax.all_gather(context, "tp", axis=1, tiled=True),
    )
    hidden = modulate(whole_lat, full_gain, full_pairs[0, 0], full_pairs[0, 1])
    hidden_ctx = modulate(whole_ctx, full_gain, full_pairs[1, 0], full_pairs[1, 1])
    query_raw = jnp.dot(hidden, w_query, preferred_element_type=jnp.float32)
    key_raw = jnp.dot(hidden, w_key, preferred_element_type=jnp.float32)
    value_raw = jnp.dot(hidden, w_value, preferred_element_type=jnp.float32)
    ctx_key_raw = jnp.dot(hidden_ctx, w_key, preferred_element_type=jnp.float32)
    ctx_value_raw = jnp.dot(hidden_ctx, w_value, preferred_element_type=jnp.float32)
    positions = lax.axis_index("sp") * tok_rows + jnp.arange(tok_rows, dtype=jnp.int32)
    queries = rotate(
        head_norm(query_raw.reshape(tok_rows, heads_here, 2, DK), query_gain), positions
    ).astype(jnp.bfloat16)
    lat_keys = (
        rotate(head_norm(key_raw.reshape(tok_rows, heads_here, 2, DK), key_gain), positions)
        .astype(jnp.bfloat16)
        .reshape(tok_rows, heads_here * 2 * DK)
    )
    lat_values = value_raw.astype(jnp.bfloat16)
    ctx_keys = (
        head_norm(ctx_key_raw.reshape(ctx_rows, heads_here, 2, DK), key_gain)
        .astype(jnp.bfloat16)
        .reshape(ctx_rows, heads_here * 2 * DK)
    )
    ctx_values = ctx_value_raw.astype(jnp.bfloat16)
    scaling = DK ** (-0.5)

    def absorb(carried, key_rows, value_rows):
        key_count = key_rows.shape[0]
        key_block = key_rows.reshape(key_count, heads_here, 2, DK)
        value_block = value_rows.reshape(key_count, heads_here, DV)
        running_max, totals, weighted = carried
        scores = (
            jnp.einsum("qhmd,khmd->qhmk", queries, key_block, preferred_element_type=jnp.float32)
            * scaling
        )
        new_max = jnp.maximum(running_max, jnp.max(scores, axis=-1))
        rescale = jnp.exp(running_max - new_max)
        exponent = jnp.exp(scores - new_max[..., None])
        totals = totals * rescale + jnp.sum(exponent, axis=-1)
        weighted = weighted * rescale[..., None] + jnp.einsum(
            "qhmk,khv->qhmv",
            exponent.astype(jnp.bfloat16),
            value_block,
            preferred_element_type=jnp.float32,
        )
        return (new_max, totals, weighted)

    def absorb_rows(carried, key_rows, value_rows):
        key_count = key_rows.shape[0]
        block_rows = math.gcd(key_count, 512)

        def visit_block(block_index, partial_value):
            first_row = block_index * block_rows
            return absorb(
                partial_value,
                lax.dynamic_slice_in_dim(key_rows, first_row, block_rows, 0),
                lax.dynamic_slice_in_dim(value_rows, first_row, block_rows, 0),
            )

        return lax.fori_loop(0, key_count // block_rows, visit_block, carried)

    initial_state = (
        jnp.full((tok_rows, heads_here, 2), -1e30, jnp.float32),
        jnp.zeros((tok_rows, heads_here, 2), jnp.float32),
        jnp.zeros((tok_rows, heads_here, 2, DV), jnp.float32),
    )
    every_ctx_keys, every_ctx_values = (
        lax.all_gather(ctx_keys, "sp", axis=0, tiled=True),
        lax.all_gather(ctx_values, "sp", axis=0, tiled=True),
    )
    carried = absorb_rows(initial_state, every_ctx_keys, every_ctx_values)
    carried = absorb_rows(
        carried,
        lax.all_gather(lat_keys, "sp", axis=0, tiled=True),
        lax.all_gather(lat_values, "sp", axis=0, tiled=True),
    )
    running_max, totals, weighted = carried
    attended = (
        weighted[:, :, 0] / totals[:, :, 0, None]
        - lambdas[None, :, None] * weighted[:, :, 1] / totals[:, :, 1, None]
    )
    head_out = head_norm(attended, out_gain).astype(jnp.bfloat16).reshape(tok_rows, heads_here * DV)
    mixed_rows = jnp.dot(
        lax.all_gather(head_out, "tp", axis=1, tiled=True),
        w_out,
        preferred_element_type=jnp.float32,
    )
    return (lat_floats + modulation[0, 2] * mixed_rows).astype(jnp.bfloat16)


def solution(mesh):
    in_specs = (
        P(("grp", "sp"), "tp"),
        P(("grp", "sp"), "tp"),
        P("grp", "sp"),
        P("sp", None, "tp"),
        P("tp"),
        P(None, "tp"),
        P(None, "tp"),
        P(None, "tp"),
        P(),
        P(),
        P("tp"),
        P(),
        P(None, "tp"),
    )
    out_specs = P(("grp", "sp"), "tp")
    return jax.shard_map(local, mesh=mesh, in_specs=in_specs, out_specs=out_specs, check_vma=False)
```

profile of v0, /device:TPU:0, one launch (start us, length us, event | category | flops | bytes accessed | tf_op | source)
XLA Modules:
  0.0 294.6 jit_solution(11514742589361231051)
XLA Ops:
  8.8 8.6 %copy.31 = bf16[1024,3,1024]{0,2,1:T(8,128)(2,1)} copy(bf16[1024,3,1024]{2,0,1:T(8,128)(2,1)} %param.20) | data formatting | bytes 12582912 | tf_op args[3]
  17.5 5.1 %fusion.27 = f32[2,3,1024]{2,0,1:T(2,128)S(1)} fusion(bf16[1024,3,1024]{0,2,1:T(8,128)(2,1)} %copy.31, f32[2,1024]{1,0:T(2,128)S(1)} %copy-done.4), kind=kOutput, calls=%fused_computation.39 | convolution fusion | flops 12593152 | bytes 6324224 | tf_op jit(solution)/shard_map/dot_general | solution.py:75
  22.5 20.6 %psum.7 = f32[2,3,1024]{2,0,1:T(2,128)S(1)} all-reduce(f32[2,3,1024]{2,0,1:T(2,128)S(1)} %fusion.27), channel_id=1, replica_groups=mesh['grp'=2,'sp'=4,'tp'=4] {'sp'}, use_global_device_ids=true, to_apply=%region_0.1 | all-reduce | flops 6144 | bytes 49152 | tf_op jit(solution)/shard_map/psum | solution.py:78
  43.2 5.2 %all_gather.28 = f32[4096]{0:T(1024)S(1)} all-gather(f32[1024]{0:T(1024)S(1)} %copy-done.7), channel_id=1, replica_groups=mesh['grp'=2,'sp'=4,'tp'=4] {'tp'}, dimensions={0}, use_global_device_ids=true | all-gather | bytes 20480 | tf_op jit(solution)/shard_map/all_gather | solution.py:81
  48.4 5.6 %all_gather.29 = f32[2,2,4096]{2,0,1:T(2,128)S(1)} all-gather(f32[2,2,1024]{2,0,1:T(2,128)S(1)} %slice.85), channel_id=1, replica_groups=mesh['grp'=2,'sp'=4,'tp'=4] {'tp'}, dimensions={2}, use_global_device_ids=true | all-gather | bytes 81920 | tf_op jit(solution)/shard_map/all_gather | solution.py:82
  54.1 2.1 fusion.29
  56.2 4.9 %convolution_convert_fusion.1 = bf16[256,512]{1,0:T(8,128)(2,1)} fusion(bf16[4096,512]{1,0:T(8,128)(2,1)} %param.24, bf16[256,4096]{1,0:T(8,128)(2,1)} %all-gather.8.cloned.1.call-done, f32[4096]{0:T(1024)S(1)} %bitcast.202, f32[4096]{0:T(1024)S(1)} %bitcast.204, f32[4096]{0:T(1024)S(1)} %all_gather.28, f32[256]{0:T(256)S(1)} %add_rsqrt_fusion.5), kind=kOutput, calls=%fused_computation.50 | convolution fusion | flops 1080164352 | bytes 6603776 | tf_op jit(solution)/shard_map/dot_general | solution.py:94
  61.4 5.0 %fusion.59 = (f32[256,512]{1,0:T(8,128)S(1)}, f32[256,512]{1,0:T(8,128)}) fusion(bf16[4096,512]{1,0:T(8,128)(2,1)} %param.23, bf16[256,4096]{1,0:T(8,128)(2,1)} %all-gather.8.cloned.1.call-done, f32[4096]{0:T(1024)S(1)} %bitcast.203, f32[4096]{0:T(1024)S(1)} %bitcast.205, f32[4096]{0:T(1024)S(1)} %all_gather.28, f32[256]{0:T(256)S(1)} %add_rsqrt_fusion.5), kind=kOutput, calls=%fused_computation.117 | convolution fusion | flops 1080164352 | bytes 7390208 | tf_op jit(solution)/shard_map/dot_general | solution.py:93
  66.9 1.9 multiply_convert_fusion
  70.7 3.2 %fusion.22 = f32[512]{0:T(512)S(1)} fusion(bf16[512,4096]{1,0:T(8,128)(2,1)} %all-gather.12.cloned.1.call-done), kind=kLoop, calls=%fused_computation.34 | loop fusion | flops 6290944 | bytes 4196352 | tf_op jit(solution)/shard_map/reduce_sum | solution.py:50
  74.1 5.4 %convolution_convert_fusion = bf16[512,512]{1,0:T(8,128)(2,1)} fusion(bf16[4096,512]{1,0:T(8,128)(2,1)} %param.24, bf16[512,4096]{1,0:T(8,128)(2,1)S(1)} %copy-done, f32[4096]{0:T(1024)S(1)} %bitcast.199, f32[4096]{0:T(1024)S(1)} %bitcast.196, f32[4096]{0:T(1024)S(1)} %all_gather.28, f32[512]{0:T(512)S(1)} %add_rsqrt_fusion.4), kind=kOutput, calls=%fused_computation.49 | convolution fusion | flops 2160328704 | bytes 8964096 | tf_op jit(solution)/shard_map/dot_general | solution.py:92
  79.8 6.4 %multiply_reduce_fusion = (f32[512,4,2]{0,2,1:T(2,128)S(1)}, f32[512,512]{0,1:T(8,128)S(1)}) fusion(bf16[4096,512]{1,0:T(8,128)(2,1)} %param.23, bf16[512,4096]{1,0:T(8,128)(2,1)} %all-gather.12.cloned.1.call-done, f32[4096]{0:T(1024)S(1)} %bitcast.200, f32[4096]{0:T(1024)S(1)} %bitcast.197, f32[4096]{0:T(1024)S(1)} %all_gather.28, f32[512]{0:T(512)S(1)} %add_rsqrt_fusion.4), kind=kOutput, calls=%fused_computation.64 | convolution fusion | flops 2160586752 | bytes 9504768 | tf_op jit(solution)/shard_map/dot_general | solution.py:91
  88.6 2.8 multiply_reduce_fusion.1
  92.2 8.0 %all-gather.14.cloned.1.call-done = bf16[1024,512]{1,0:T(8,128)(2,1)} async-done(((bf16[256,512]{1,0:T(8,128)(2,1)}), bf16[1024,512]{1,0:T(8,128)(2,1)}) %all-gather.14.cloned.1.call-update) | async-done | bytes 1048592 | tf_op jit(solution)/shard_map/all_gather | solution.py:155
  100.2 28.8 %all-gather.10.cloned.1.call-done = bf16[1024,512]{1,0:T(8,128)(2,1)} async-done(((bf16[256,512]{1,0:T(8,128)(2,1)}), bf16[1024,512]{1,0:T(8,128)(2,1)}) %all-gather.10.cloned.1.call-update) | async-done | bytes 1048592 | tf_op jit(solution)/shard_map/all_gather | solution.py:154
  129.0 20.6 %while.36 = (s32[]{:T(128)}, f32[512,4,2]{0,2,1:T(2,128)S(1)}, f32[512,4,2]{0,2,1:T(2,128)S(1)}, f32[512,4,2,128]{0,3,2,1:T(8,128)S(1)}, bf16[1024,512]{1,0:T(8,...) while((s32[]{:T(128)}, f32[512,4,2]{0,2,1:T(2,128)S(1)}, ...), condition=%wide.region_8.9_spmd.clone, body=%wide.region_5.8_spmd.clone.sunk | while | flops 823676928 | bytes 35389616 | solution.py:146
  129.0 2.1 constant_dynamic-slice_fusion.9
  132.1 1.3 copy.58
  133.3 2.4 bitcast_reduce_fusion.6
  135.7 1.4 fusion.96
  137.2 2.1 bitcast_add_fusion.5
  139.3 2.1 constant_dynamic-slice_fusion.9
  142.4 1.3 copy.58
  143.7 2.4 bitcast_reduce_fusion.6
  146.1 1.4 fusion.96
  147.5 2.1 bitcast_add_fusion.5
  149.7 25.8 %all-gather.18.cloned.1.call-done = bf16[2048,512]{1,0:T(8,128)(2,1)} async-done(((bf16[512,512]{1,0:T(8,128)(2,1)}), bf16[2048,512]{1,0:T(8,128)(2,1)}) %all-gather.18.cloned.1.call-update) | async-done | bytes 2097168 | tf_op jit(solution)/shard_map/all_gather | solution.py:161
  175.5 45.9 %all-gather.16.cloned.1.call-done = bf16[2048,512]{0,1:T(8,128)(2,1)} async-done(((bf16[512,512]{0,1:T(8,128)(2,1)}), bf16[2048,512]{0,1:T(8,128)(2,1)}) %all-gather.16.cloned.1.call-update) | async-done | bytes 2097168 | tf_op jit(solution)/shard_map/all_gather | solution.py:160
  221.4 36.4 %while.35 = (s32[]{:T(128)}, f32[512,4,2]{0,2,1:T(2,128)S(1)}, f32[512,4,2]{0,2,1:T(2,128)S(1)}, f32[512,4,2,128]{0,3,2,1:T(8,128)S(1)}, bf16[2048,512]{0,1:T(8,...) while((s32[]{:T(128)}, f32[512,4,2]{0,2,1:T(2,128)S(1)}, ...), condition=%wide.region_13.14_spmd, body=%wide.region_10.13_spmd.sunk | while | flops 823140352 | bytes 34341024 | solution.py:146
  221.4 1.9 constant_dynamic-slice_fusion.8
  223.3 1.3 copy.56
  225.6 1.3 bitcast_reduce_fusion.5
  227.0 1.4 fusion.90
  228.4 2.1 bitcast_add_fusion.4
  230.5 1.9 constant_dynamic-slice_fusion.8
  234.7 1.3 bitcast_reduce_fusion.5
  236.1 1.4 fusion.90
  237.5 2.1 bitcast_add_fusion.4
  239.6 1.9 constant_dynamic-slice_fusion.8
  243.9 1.3 bitcast_reduce_fusion.5
  245.2 1.4 fusion.90
  246.6 2.1 bitcast_add_fusion.4
  248.8 1.9 constant_dynamic-slice_fusion.8
  253.0 1.3 bitcast_reduce_fusion.5
  254.3 1.4 fusion.90
  255.7 2.1 bitcast_add_fusion.4
  260.8 20.8 %all-gather.20.cloned.1.call-done = bf16[512,2048]{0,1:T(8,128)(2,1)} async-done(((bf16[512,512]{0,1:T(8,128)(2,1)}), bf16[512,2048]{0,1:T(8,128)(2,1)}) %all-gather.20.cloned.1.call-update) | async-done | bytes 2097168 | tf_op jit(solution)/shard_map/all_gather | solution.py:170
  281.6 6.1 %add_convert_fusion = bf16[512,1024]{1,0:T(8,128)(2,1)} fusion(bf16[512,1024]{1,0:T(8,128)(2,1)S(1)} %copy-done.2, bf16[512,2048]{0,1:T(8,128)(2,1)} %all-gather.20.cloned.1.call-done, bf16[2048,1024]{1,0:T(8,128)(2,1)} %param.29, f32[1024]{0:T(1024)S(1)} %bitcast.206), kind=kOutput, calls=%fused_computation.48 | convolution fusion | flops 2149580800 | bytes 8392704 | tf_op jit(solution)/shard_map/dot_general | solution.py:169
  (107 shorter events, 21.9 us)
Async XLA Ops:
  6.5 47.5 %all-gather.8.cloned.1.call-start = ((), (), s32[]{:S(2)}) async-start(), calls=%async_computation | async-start | bytes 2621440 | tf_op jit(solution)/shard_map/all_gather | solution.py:86
  7.3 63.4 %all-gather.12.cloned.1.call-start = ((), (), s32[]{:S(2)}) async-start(), calls=%async_computation.2 | async-start | bytes 5242880 | tf_op jit(solution)/shard_map/all_gather | solution.py:85
  8.0 92.2 %all-gather.14.cloned.1.call-start = ((), (), s32[]{:S(2)}) async-start(), calls=%async_computation.3 | async-start | bytes 1310720 | tf_op jit(solution)/shard_map/all_gather | solution.py:155
  8.8 8.7 %copy-start.4 = (f32[2,1024]{1,0:T(2,128)S(1)}, f32[2,1024]{1,0:T(2,128)}, u32[]{:S(2)}) copy-start(f32[2,1024]{1,0:T(2,128)} %param.19) | copy-start | bytes 24580
  17.5 25.7 %copy-start.7 = (f32[1024]{0:T(1024)S(1)}, f32[1024]{0:T(1024)}, u32[]{:S(2)}) copy-start(f32[1024]{0:T(1024)} %param.21) | copy-start | bytes 12292
  43.1 17.9 %copy-start.3 = (f32[2,3,1024]{2,0,1:T(2,128)}, f32[2,3,1024]{2,0,1:T(2,128)S(1)}, u32[]{:S(2)}) copy-start(f32[2,3,1024]{2,0,1:T(2,128)S(1)} %psum.7) | copy-start | bytes 73732
  61.0 68.0 %all-gather.10.cloned.1.call-start = ((), (), s32[]{:S(2)}) async-start(), calls=%async_computation.1 | async-start | bytes 1310720 | tf_op jit(solution)/shard_map/all_gather | solution.py:154
  66.4 2.5 copy-start.9
  66.4 2.5 copy-start.12
  68.8 106.7 %all-gather.18.cloned.1.call-start = ((), (), s32[]{:S(2)}) async-start(), calls=%async_computation.5 | async-start | bytes 2621440 | tf_op jit(solution)/shard_map/all_gather | solution.py:161
  70.7 3.4 %copy-start = (bf16[512,4096]{1,0:T(8,128)(2,1)S(1)}, bf16[512,4096]{1,0:T(8,128)(2,1)}, u32[]{:S(2)}) copy-start(bf16[512,4096]{1,0:T(8,128)(2,1)} %all-gather.12.cloned.1.call-done) | copy-start | bytes 12582916
  79.5 6.7 %copy-start.8 = (f32[64]{0:T(128)S(1)}, f32[64]{0:T(128)}, u32[]{:S(2)}) copy-start(f32[64]{0:T(128)} %param.26) | copy-start | bytes 772
  79.5 141.9 %all-gather.16.cloned.1.call-start = ((), (), s32[]{:S(2)}) async-start(), calls=%async_computation.4 | async-start | bytes 2621440 | tf_op jit(solution)/shard_map/all_gather | solution.py:160
  79.8 7.7 %copy-start.13 = (bf16[4096,512]{1,0:T(8,128)(2,1)S(1)}, bf16[4096,512]{1,0:T(8,128)(2,1)}, u32[]{:S(2)}) copy-start(bf16[4096,512]{1,0:T(8,128)(2,1)} %param.22) | copy-start | bytes 12582916
  86.2 2.4 copy-start.1
  88.6 2.8 copy-start.11
  91.9 189.7 %all-gather.20.cloned.1.call-start = ((), (), s32[]{:S(2)}) async-start(), calls=%async_computation.6 | async-start | bytes 2621440 | tf_op jit(solution)/shard_map/all_gather | solution.py:170
  257.9 0.7 copy-start.10
  258.0 1.0 copy-start.5
  258.0 1.0 copy-start.6
  258.2 23.4 %copy-start.2 = (bf16[512,1024]{1,0:T(8,128)(2,1)S(1)}, bf16[512,1024]{1,0:T(8,128)(2,1)}, u32[]{:S(2)}) copy-start(bf16[512,1024]{1,0:T(8,128)(2,1)} %param.17) | copy-start | bytes 3145732
Sparse Core Ops, SparseCore 0:
  8.9 25.2 all-gather.7
  35.8 34.8 all-gather.11
  72.3 27.8 all-gather.13
  101.6 27.3 all-gather.9
  130.4 45.0 all-gather.17
  176.9 44.4 all-gather.15
  260.2 21.3 all-gather.19
where the time goes:
time: 296 us; the launch traced here: 295 us
  waiting for transfers between devices  132 us (45%)
  matrix products  58.2 us (20%)
  local copies, waits for them, and re-layouts  38.6 us (13%)
  blocking collectives  31.4 us (11%)
  other arithmetic  19.5 us (7%)
  between operations  13.9 us (5%)
    all_gather x1, waiting for transfers between devices, local(): lax.all_gather(lat_keys, 'sp', axis=0, tiled=True)  45.9 us
    all_gather x1, waiting for transfers between devices, local(): lax.all_gather(ctx_keys, 'sp', axis=0, tiled=True)  28.8 us
    all_gather x1, waiting for transfers between devices, local(): lax.all_gather(lat_values, 'sp', axis=0, tiled=True)  25.8 us
    all_gather x1, waiting for transfers between devices, local(): lax.all_gather(head_out, 'tp', axis=1, tiled=True)  20.8 us
    psum x1, blocking collectives, local(): modulation = lax.psum(partial_mod, 'sp')  20.6 us
    dynamic_slice x12, local copies, waits for them, and re-layouts, visit_block(): lax.dynamic_slice_in_dim(value_rows, first_row, block_rows, 0)  19.1 us
    dot_general x6, matrix products, absorb(): jnp.einsum('qhmk,khv->qhmv', exponent.astype(jnp.bfloat16), value_block,...  12.7 us
    unnamed x31, local copies, waits for them, and re-layouts  10.2 us
  transfers between devices with their start and end apart: 7, of which 6 were waited for; matrix products, arithmetic and copies ran while one was open for 24% of the time, Pallas kernels for 0%

commit v1 on v0

--- a/solution.py
+++ b/solution.py
@@ -75,7 +75,7 @@
     partial_mod = jnp.dot(
         activated, mod_weight.reshape(in_rows, 3 * columns), preferred_element_type=jnp.float32
     ).reshape(2, 3, columns)
-    modulation = lax.psum(partial_mod, "sp")
+    modulation = jnp.sum(lax.all_gather(partial_mod, "sp"), axis=0)
     lat_floats = latent.astype(jnp.float32)
     full_gain, full_pairs = (
         lax.all_gather(norm_gain, "tp", axis=0, tiled=True),

time: 296 us -> 296 us (level)
  waiting for transfers between devices: 132 us -> 138 us
  blocking collectives: 31.4 us -> 25.5 us
    psum x1 -> x0, blocking collectives: 20.6 us -> none  [local(): modulation = lax.psum(partial_mod, 'sp')]
    all_gather x0 -> x1, blocking collectives: none -> 14.9 us  [local(): modulation = jnp.sum(lax.all_gather(partial_mod, 'sp'), axis=0)]
    all_gather x1, waiting for transfers between devices: 1.18 us -> 6.92 us  [local(): lax.all_gather(latent, 'tp', axis=1, tiled=True)]
    unnamed x31 -> x32, local copies, waits for them, and re-layouts: 10.2 us -> 10.2 us
where the time goes in v1:
time: 296 us; the launch traced here: 295 us
  waiting for transfers between devices  138 us (47%)
  matrix products  58.2 us (20%)
  local copies, waits for them, and re-layouts  38.7 us (13%)
  blocking collectives  25.5 us (9%)
  other arithmetic  19.5 us (7%)
  between operations  13.9 us (5%)
    all_gather x1, waiting for transfers between devices, local(): lax.all_gather(lat_keys, 'sp', axis=0, tiled=True)  45.9 us
    all_gather x1, waiting for transfers between devices, local(): lax.all_gather(ctx_keys, 'sp', axis=0, tiled=True)  28.8 us
    all_gather x1, waiting for transfers between devices, local(): lax.all_gather(lat_values, 'sp', axis=0, tiled=True)  25.8 us
    all_gather x1, waiting for transfers between devices, local(): lax.all_gather(head_out, 'tp', axis=1, tiled=True)  20.8 us
    dynamic_slice x12, local copies, waits for them, and re-layouts, visit_block(): lax.dynamic_slice_in_dim(value_rows, first_row, block_rows, 0)  19.1 us
    all_gather x1, blocking collectives, local(): modulation = jnp.sum(lax.all_gather(partial_mod, 'sp'), axis=0)  14.9 us
    dot_general x6, matrix products, absorb(): jnp.einsum('qhmk,khv->qhmv', exponent.astype(jnp.bfloat16), value_block,...  12.7 us
    unnamed x32, local copies, waits for them, and re-layouts  10.2 us
  transfers between devices with their start and end apart: 7, of which 6 were waited for; matrix products, arithmetic and copies ran while one was open for 24% of the time, Pallas kernels for 0%

profile of v1, /device:TPU:0, one launch (start us, length us, event | category | flops | bytes accessed | tf_op | source)
XLA Modules:
  0.0 294.6 jit_solution(4935454092314804268)
XLA Ops:
  8.8 8.6 %copy.31 = bf16[1024,3,1024]{0,2,1:T(8,128)(2,1)} copy(bf16[1024,3,1024]{2,0,1:T(8,128)(2,1)} %param.20) | data formatting | bytes 12582912 | tf_op args[3]
  17.5 5.1 %fusion.27 = f32[2,3,1024]{2,0,1:T(2,128)S(1)} fusion(bf16[1024,3,1024]{0,2,1:T(8,128)(2,1)} %copy.31, f32[2,1024]{1,0:T(2,128)S(1)} %copy-done.4), kind=kOutput, calls=%fused_computation.39 | convolution fusion | flops 12593152 | bytes 6324224 | tf_op jit(solution)/shard_map/dot_general | solution.py:75
  22.6 14.9 %all-gather = f32[8,3,1024]{2,1,0:T(4,128)S(1)} all-gather(f32[2,3,1024]{2,1,0:T(4,128)S(1)} %copy.32), channel_id=2, replica_groups=mesh['grp'=2,'sp'=4,'tp'=4] {'sp'}, dimensions={0}, use_global_device_ids=true | all-gather | bytes 122880 | tf_op jit(solution)/shard_map/all_gather | solution.py:78
  37.6 5.2 %all_gather.32 = f32[4096]{0:T(1024)S(1)} all-gather(f32[1024]{0:T(1024)S(1)} %copy-done.7), channel_id=1, replica_groups=mesh['grp'=2,'sp'=4,'tp'=4] {'tp'}, dimensions={0}, use_global_device_ids=true | all-gather | bytes 20480 | tf_op jit(solution)/shard_map/all_gather | solution.py:81
  42.8 5.4 %all_gather.33 = f32[2,2,4096]{2,0,1:T(2,128)S(1)} all-gather(f32[2,2,1024]{2,0,1:T(2,128)S(1)} %copy.50), channel_id=1, replica_groups=mesh['grp'=2,'sp'=4,'tp'=4] {'tp'}, dimensions={2}, use_global_device_ids=true | all-gather | bytes 81920 | tf_op jit(solution)/shard_map/all_gather | solution.py:82
  48.2 2.1 fusion.29
  50.3 4.9 %convolution_convert_fusion.1 = bf16[256,512]{1,0:T(8,128)(2,1)} fusion(bf16[4096,512]{1,0:T(8,128)(2,1)} %param.24, bf16[256,4096]{1,0:T(8,128)(2,1)} %all-gather.9.cloned.1.call-done, f32[4096]{0:T(1024)S(1)} %bitcast.206, f32[4096]{0:T(1024)S(1)} %bitcast.208, f32[4096]{0:T(1024)S(1)} %all_gather.32, f32[256]{0:T(256)S(1)} %add_rsqrt_fusion.5), kind=kOutput, calls=%fused_computation.50 | convolution fusion | flops 1080164352 | bytes 6603776 | tf_op jit(solution)/shard_map/dot_general | solution.py:94
  55.6 4.9 %fusion.59 = (f32[256,512]{1,0:T(8,128)S(1)}, f32[256,512]{1,0:T(8,128)}) fusion(bf16[4096,512]{1,0:T(8,128)(2,1)} %param.23, bf16[256,4096]{1,0:T(8,128)(2,1)} %all-gather.9.cloned.1.call-done, f32[4096]{0:T(1024)S(1)} %bitcast.207, f32[4096]{0:T(1024)S(1)} %bitcast.209, f32[4096]{0:T(1024)S(1)} %all_gather.32, f32[256]{0:T(256)S(1)} %add_rsqrt_fusion.5), kind=kOutput, calls=%fused_computation.117 | convolution fusion | flops 1080164352 | bytes 7390208 | tf_op jit(solution)/shard_map/dot_general | solution.py:93
  61.1 1.9 multiply_convert_fusion
  63.7 6.9 %all-gather.13.cloned.1.call-done = bf16[512,4096]{1,0:T(8,128)(2,1)} async-done(((bf16[512,1024]{1,0:T(8,128)(2,1)}), bf16[512,4096]{1,0:T(8,128)(2,1)}) %all-gather.13.cloned.1.call-update) | async-done | bytes 4194320 | tf_op jit(solution)/shard_map/all_gather | solution.py:85
  70.6 3.2 %fusion.22 = f32[512]{0:T(512)S(1)} fusion(bf16[512,4096]{1,0:T(8,128)(2,1)} %all-gather.13.cloned.1.call-done), kind=kLoop, calls=%fused_computation.34 | loop fusion | flops 6290944 | bytes 4196352 | tf_op jit(solution)/shard_map/reduce_sum | solution.py:50
  74.1 5.4 %convolution_convert_fusion = bf16[512,512]{1,0:T(8,128)(2,1)} fusion(bf16[4096,512]{1,0:T(8,128)(2,1)} %param.24, bf16[512,4096]{1,0:T(8,128)(2,1)S(1)} %copy-done, f32[4096]{0:T(1024)S(1)} %bitcast.203, f32[4096]{0:T(1024)S(1)} %bitcast.200, f32[4096]{0:T(1024)S(1)} %all_gather.32, f32[512]{0:T(512)S(1)} %add_rsqrt_fusion.4), kind=kOutput, calls=%fused_computation.49 | convolution fusion | flops 2160328704 | bytes 8964096 | tf_op jit(solution)/shard_map/dot_general | solution.py:92
  79.7 6.4 %multiply_reduce_fusion = (f32[512,4,2]{0,2,1:T(2,128)S(1)}, f32[512,512]{0,1:T(8,128)S(1)}) fusion(bf16[4096,512]{1,0:T(8,128)(2,1)} %param.23, bf16[512,4096]{1,0:T(8,128)(2,1)} %all-gather.13.cloned.1.call-done, f32[4096]{0:T(1024)S(1)} %bitcast.204, f32[4096]{0:T(1024)S(1)} %bitcast.201, f32[4096]{0:T(1024)S(1)} %all_gather.32, f32[512]{0:T(512)S(1)} %add_rsqrt_fusion.4), kind=kOutput, calls=%fused_computation.64 | convolution fusion | flops 2160586752 | bytes 9504768 | tf_op jit(solution)/shard_map/dot_general | solution.py:91
  88.5 2.8 multiply_reduce_fusion.1
  92.1 8.1 %all-gather.15.cloned.1.call-done = bf16[1024,512]{1,0:T(8,128)(2,1)} async-done(((bf16[256,512]{1,0:T(8,128)(2,1)}), bf16[1024,512]{1,0:T(8,128)(2,1)}) %all-gather.15.cloned.1.call-update) | async-done | bytes 1048592 | tf_op jit(solution)/shard_map/all_gather | solution.py:155
  100.2 28.8 %all-gather.11.cloned.1.call-done = bf16[1024,512]{1,0:T(8,128)(2,1)} async-done(((bf16[256,512]{1,0:T(8,128)(2,1)}), bf16[1024,512]{1,0:T(8,128)(2,1)}) %all-gather.11.cloned.1.call-update) | async-done | bytes 1048592 | tf_op jit(solution)/shard_map/all_gather | solution.py:154
  129.0 20.6 %while.36 = (s32[]{:T(128)}, f32[512,4,2]{0,2,1:T(2,128)S(1)}, f32[512,4,2]{0,2,1:T(2,128)S(1)}, f32[512,4,2,128]{0,3,2,1:T(8,128)S(1)}, bf16[1024,512]{1,0:T(8,...) while((s32[]{:T(128)}, f32[512,4,2]{0,2,1:T(2,128)S(1)}, ...), condition=%wide.region_8.9_spmd.clone, body=%wide.region_5.8_spmd.clone.sunk | while | flops 823676928 | bytes 35389616 | solution.py:146
  129.0 2.1 constant_dynamic-slice_fusion.9
  132.1 1.3 copy.63
  133.3 2.4 bitcast_reduce_fusion.6
  135.7 1.4 fusion.96
  137.2 2.1 bitcast_add_fusion.5
  139.3 2.1 constant_dynamic-slice_fusion.9
  142.4 1.3 copy.63
  143.7 2.4 bitcast_reduce_fusion.6
  146.1 1.4 fusion.96
  147.5 2.1 bitcast_add_fusion.5
  149.7 25.8 %all-gather.19.cloned.1.call-done = bf16[2048,512]{1,0:T(8,128)(2,1)} async-done(((bf16[512,512]{1,0:T(8,128)(2,1)}), bf16[2048,512]{1,0:T(8,128)(2,1)}) %all-gather.19.cloned.1.call-update) | async-done | bytes 2097168 | tf_op jit(solution)/shard_map/all_gather | solution.py:161
  175.5 45.9 %all-gather.17.cloned.1.call-done = bf16[2048,512]{0,1:T(8,128)(2,1)} async-done(((bf16[512,512]{0,1:T(8,128)(2,1)}), bf16[2048,512]{0,1:T(8,128)(2,1)}) %all-gather.17.cloned.1.call-update) | async-done | bytes 2097168 | tf_op jit(solution)/shard_map/all_gather | solution.py:160
  221.4 36.4 %while.35 = (s32[]{:T(128)}, f32[512,4,2]{0,2,1:T(2,128)S(1)}, f32[512,4,2]{0,2,1:T(2,128)S(1)}, f32[512,4,2,128]{0,3,2,1:T(8,128)S(1)}, bf16[2048,512]{0,1:T(8,...) while((s32[]{:T(128)}, f32[512,4,2]{0,2,1:T(2,128)S(1)}, ...), condition=%wide.region_13.14_spmd, body=%wide.region_10.13_spmd.sunk | while | flops 823140352 | bytes 34341024 | solution.py:146
  221.4 1.9 constant_dynamic-slice_fusion.8
  225.6 1.3 bitcast_reduce_fusion.5
  227.0 1.4 fusion.90
  228.4 2.1 bitcast_add_fusion.4
  230.5 1.9 constant_dynamic-slice_fusion.8
  234.7 1.3 bitcast_reduce_fusion.5
  236.1 1.4 fusion.90
  237.5 2.1 bitcast_add_fusion.4
  239.6 1.9 constant_dynamic-slice_fusion.8
  243.9 1.3 bitcast_reduce_fusion.5
  245.2 1.4 fusion.90
  246.6 2.1 bitcast_add_fusion.4
  248.8 1.9 constant_dynamic-slice_fusion.8
  253.0 1.3 bitcast_reduce_fusion.5
  254.3 1.4 fusion.90
  255.7 2.1 bitcast_add_fusion.4
  260.8 20.8 %all-gather.21.cloned.1.call-done = bf16[512,2048]{0,1:T(8,128)(2,1)} async-done(((bf16[512,512]{0,1:T(8,128)(2,1)}), bf16[512,2048]{0,1:T(8,128)(2,1)}) %all-gather.21.cloned.1.call-update) | async-done | bytes 2097168 | tf_op jit(solution)/shard_map/all_gather | solution.py:170
  281.6 6.1 %add_convert_fusion = bf16[512,1024]{1,0:T(8,128)(2,1)} fusion(bf16[512,1024]{1,0:T(8,128)(2,1)S(1)} %copy-done.2, bf16[512,2048]{0,1:T(8,128)(2,1)} %all-gather.21.cloned.1.call-done, bf16[2048,1024]{1,0:T(8,128)(2,1)} %param.29, f32[1024]{0:T(1024)S(1)} %bitcast.210), kind=kOutput, calls=%fused_computation.48 | convolution fusion | flops 2149580800 | bytes 8392704 | tf_op jit(solution)/shard_map/dot_general | solution.py:169
  (110 shorter events, 22.0 us)
Async XLA Ops:
  6.5 41.7 %all-gather.9.cloned.1.call-start = ((), (), s32[]{:S(2)}) async-start(), calls=%async_computation | async-start | bytes 2621440 | tf_op jit(solution)/shard_map/all_gather | solution.py:86
  7.3 63.4 %all-gather.13.cloned.1.call-start = ((), (), s32[]{:S(2)}) async-start(), calls=%async_computation.2 | async-start | bytes 5242880 | tf_op jit(solution)/shard_map/all_gather | solution.py:85
  8.0 92.2 %all-gather.15.cloned.1.call-start = ((), (), s32[]{:S(2)}) async-start(), calls=%async_computation.3 | async-start | bytes 1310720 | tf_op jit(solution)/shard_map/all_gather | solution.py:155
  8.8 8.7 %copy-start.4 = (f32[2,1024]{1,0:T(2,128)S(1)}, f32[2,1024]{1,0:T(2,128)}, u32[]{:S(2)}) copy-start(f32[2,1024]{1,0:T(2,128)} %param.19) | copy-start | bytes 24580
  17.5 20.1 %copy-start.7 = (f32[1024]{0:T(1024)S(1)}, f32[1024]{0:T(1024)}, u32[]{:S(2)}) copy-start(f32[1024]{0:T(1024)} %param.21) | copy-start | bytes 12292
  37.5 17.7 %copy-start.3 = (f32[2,3,1024]{2,1,0:T(4,128)}, f32[2,3,1024]{2,1,0:T(4,128)S(1)}, u32[]{:S(2)}) copy-start(f32[2,3,1024]{2,1,0:T(4,128)S(1)} %reduce_sum.89) | copy-start | bytes 73732
  55.2 73.8 %all-gather.11.cloned.1.call-start = ((), (), s32[]{:S(2)}) async-start(), calls=%async_computation.1 | async-start | bytes 1310720 | tf_op jit(solution)/shard_map/all_gather | solution.py:154
  60.5 2.5 copy-start.9
  60.5 2.5 copy-start.12
  63.0 112.5 %all-gather.19.cloned.1.call-start = ((), (), s32[]{:S(2)}) async-start(), calls=%async_computation.5 | async-start | bytes 2621440 | tf_op jit(solution)/shard_map/all_gather | solution.py:161
  70.6 3.4 %copy-start = (bf16[512,4096]{1,0:T(8,128)(2,1)S(1)}, bf16[512,4096]{1,0:T(8,128)(2,1)}, u32[]{:S(2)}) copy-start(bf16[512,4096]{1,0:T(8,128)(2,1)} %all-gather.13.cloned.1.call-done) | copy-start | bytes 12582916
  79.4 6.7 %copy-start.8 = (f32[64]{0:T(128)S(1)}, f32[64]{0:T(128)}, u32[]{:S(2)}) copy-start(f32[64]{0:T(128)} %param.26) | copy-start | bytes 772
  79.5 142.0 %all-gather.17.cloned.1.call-start = ((), (), s32[]{:S(2)}) async-start(), calls=%async_computation.4 | async-start | bytes 2621440 | tf_op jit(solution)/shard_map/all_gather | solution.py:160
  79.7 7.7 %copy-start.13 = (bf16[4096,512]{1,0:T(8,128)(2,1)S(1)}, bf16[4096,512]{1,0:T(8,128)(2,1)}, u32[]{:S(2)}) copy-start(bf16[4096,512]{1,0:T(8,128)(2,1)} %param.22) | copy-start | bytes 12582916
  86.1 2.4 copy-start.1
  88.5 2.8 copy-start.11
  91.8 189.8 %all-gather.21.cloned.1.call-start = ((), (), s32[]{:S(2)}) async-start(), calls=%async_computation.6 | async-start | bytes 2621440 | tf_op jit(solution)/shard_map/all_gather | solution.py:170
  257.9 0.7 copy-start.10
  258.0 1.0 copy-start.5
  258.0 1.0 copy-start.6
  258.2 23.4 %copy-start.2 = (bf16[512,1024]{1,0:T(8,128)(2,1)S(1)}, bf16[512,1024]{1,0:T(8,128)(2,1)}, u32[]{:S(2)}) copy-start(bf16[512,1024]{1,0:T(8,128)(2,1)} %param.17) | copy-start | bytes 3145732
Sparse Core Ops, SparseCore 0:
  8.9 25.2 all-gather.8
  35.8 34.7 all-gather.12
  72.2 27.9 all-gather.14
  101.6 27.3 all-gather.10
  130.4 45.0 all-gather.18
  176.9 44.4 all-gather.16
  260.2 21.3 all-gather.20
